TPU v7x, 32 devices: a whole 2x2x4 slice. The times are simulated.
32 devices in a mesh: ep: 8 (over z, core), tp: 4 (over y, x).
Axes of the slice: x: 2, y: 2, z: 4, core: 2. Of those that a mesh axis runs over, the one named last changes fastest.
Arguments:
- tokens: bfloat16 [1024, 2048], P('ep', 'tp'), may hold values from -6 to 6
- routing: int32 [1024, 2], P('ep'), may hold values from 0 to 3, all different within a row; in each aligned block of 128 rows (0 to 127, 128 to 255, ...) at most 80 rows name the same one
- mixing: float32 [1024, 2], P('ep'), may hold values from 0.1 to 0.9
- gate_matrix: bfloat16 [8, 2048, 2048], P('ep', None, 'tp'), may hold values from -0.125 to 0.125
- up_matrix: bfloat16 [8, 2048, 2048], P('ep', None, 'tp'), may hold values from -0.125 to 0.125
- down_matrix: bfloat16 [8, 2048, 2048], P('ep', 'tp'), may hold values from -0.09375 to 0.09375
- upstream: bfloat16 [1024, 2048], P('ep', 'tp'), may hold values from -6 to 6
Outputs:
- token_gradient: bfloat16 [1024, 2048], P('ep', 'tp')
- mixing_gradient: float32 [1024, 2], P('ep')
- gate_gradient: bfloat16 [8, 2048, 2048], P('ep', None, 'tp')
- up_gradient: bfloat16 [8, 2048, 2048], P('ep', None, 'tp')
- down_gradient: bfloat16 [8, 2048, 2048], P('ep', 'tp')
- input_norms: float32 [8, 2, 2048], P('ep')
- down_norms: float32 [8, 2048], P('ep', 'tp')
Inputs may be any that keep to these rules, and one draw needn't show every extreme that they name: `routing`: A token's 2 experts differ. In each aligned block of 128 rows (the rows of one index of ep) no expert is named by more than 80 rows, and in every draw some expert is named by exactly 80 rows of some block.
All inputs are finite; a program needn't handle non-finite values.
Results may differ from a plain program's by a relative error of at most 0.0064.
Values may be sent and summed in bfloat16 or wider, within the bound.
A program may use at most 64 MiB of HBM per device.

v0:
```python
import functools

import jax
import jax.numpy as jnp
from jax import lax
from jax.experimental import pallas as pl
from jax.experimental.pallas import tpu as pltpu
from jax.sharding import PartitionSpec as P

MESH = pl.DeviceIdType.MESH
F32 = jnp.float32
BF16 = jnp.bfloat16


def send(src, dst, send_sem, recv_sem, ep, tp):
    copy = pltpu.make_async_remote_copy(
        src_ref=src, dst_ref=dst, send_sem=send_sem, recv_sem=recv_sem,
        device_id=(ep, tp), device_id_type=MESH,
    )
    copy.start()
    return copy


def arrived(ref, sem):
    pltpu.make_async_copy(ref, ref, sem).wait()


def places():
    ep, tp = lax.axis_index("ep"), lax.axis_index("tp")
    return ep // 2, ep % 2, tp


def tp_peer(tp, step, n_tp):
    if n_tp == 4:
        x, y = tp % 2, tp // 2
        return ((1 - y) if step // 2 else y) * 2 + ((1 - x) if step % 2 else x)
    return (tp + step) % n_tp


def tp_from(tp, step, n_tp):
    if n_tp == 4:
        return tp_peer(tp, step, n_tp)
    return (tp + n_tp - step) % n_tp


def greet(zs, n_tp, z, c, t):
    barrier = pltpu.get_barrier_semaphore()
    for k in range(1, zs):
        pl.semaphore_signal(barrier, inc=1, device_id=((z + k) % zs * 2 + c, t), device_id_type=MESH)
    for k in range(1, n_tp):
        pl.semaphore_signal(barrier, inc=1, device_id=(z * 2 + c, (t + k) % n_tp), device_id_type=MESH)
    pl.semaphore_signal(barrier, inc=1, device_id=(z * 2 + 1 - c, t), device_id_type=MESH)
    pl.semaphore_wait(barrier, zs + n_tp - 1)


def distances(zs):
    order = []
    for k in range(1, zs // 2 + 1):
        order.append(k)
        if zs - k != k:
            order.append(zs - k)
    return order


def dispatch_kernel(
    zs, n_tp, part, x_in, y_in, x_out, y_out, ep_send, ep_recv, tp_send, tp_recv,
    fwd_send, core_send, core_recv,
):
    z, c, t = places()
    chunks = zs if zs <= 4 else 1
    span = zs // chunks
    ins, outs = (x_in, y_in), (x_out, y_out)
    greet(zs, n_tp, z, c, t)

    def block(a, core, q, feat):
        cols = pl.ds(pl.multiple_of(feat * part, part), part)
        return outs[a].at[core, pl.ds(q * span, span), :, cols]

    def mine(a):
        cols = pl.ds(pl.multiple_of(t * part, part), part)
        return outs[a].at[c, z, :, cols]

    sent = []
    home = z // span
    for a in range(2):
        pltpu.make_async_copy(ins[a].at[z], mine(a), ep_recv.at[a, home]).start()
    for k in distances(zs):
        for a in range(2):
            dest = (z + k) % zs
            sent.append(send(ins[a].at[dest], mine(a), ep_send.at[a, k], ep_recv.at[a, home], dest * 2 + c, t))

    direct = (1, 2) if n_tp == 4 else range(1, n_tp)

    def to_core(a, q, feat):
        ref = block(a, c, q, feat)
        sent.append(send(ref, ref, core_send.at[a, q, feat], core_recv.at[a, q, feat], z * 2 + 1 - c, t))

    def spread(q):
        for a in range(2):
            ref = block(a, c, q, t)
            arrived(ref, ep_recv.at[a, q])
            for s in direct:
                sent.append(send(ref, ref, tp_send.at[a, q, s], tp_recv.at[a, q, t], z * 2 + c, tp_peer(t, s, n_tp)))
            to_core(a, q, t)

    def relay(q):
        if n_tp == 4:
            for a, s in ((0, 1), (1, 2), (1, 1), (0, 2)):
                feat = tp_from(t, s, n_tp)
                ref = block(a, c, q, feat)
                arrived(ref, tp_recv.at[a, q, feat])
                if s == a + 1:
                    sent.append(send(ref, ref, fwd_send.at[a, q], tp_recv.at[a, q, feat], z * 2 + c, tp_peer(t, 3 - s, n_tp)))
                to_core(a, q, feat)
        else:
            for s in direct:
                feat = tp_from(t, s, n_tp)
                for a in range(2):
                    arrived(block(a, c, q, feat), tp_recv.at[a, q, feat])
                    to_core(a, q, feat)

    def finish(q):
        if n_tp == 4:
            feat = tp_from(t, 3, n_tp)
            for a in range(2):
                arrived(block(a, c, q, feat), tp_recv.at[a, q, feat])
                to_core(a, q, feat)

    if chunks == 1:
        order = [0]
    else:
        order = [z] + [(z + zs - k) % zs for k in distances(zs)]
    for i in range(chunks + 2):
        if i < chunks:
            spread(order[i])
        if 1 <= i <= chunks:
            relay(order[i - 1])
        if i >= 2:
            finish(order[i - 2])
    for a in range(2):
        for q in range(chunks):
            for feat in range(n_tp):
                arrived(block(a, 1 - c, q, feat), core_recv.at[a, q, feat])
    for copy in sent:
        copy.wait_send()


def dispatch(x, y, zs, n_tp):
    _, cap, part = x.shape
    chunks = zs if zs <= 4 else 1
    out = jax.ShapeDtypeStruct((2, zs, cap, n_tp * part), BF16)
    vm = pl.BlockSpec(memory_space=pltpu.VMEM)
    dma = pltpu.SemaphoreType.DMA
    return pl.pallas_call(
        functools.partial(dispatch_kernel, zs, n_tp, part),
        out_shape=(out, out),
        in_specs=[vm, vm],
        out_specs=(vm, vm),
        scratch_shapes=[
            dma((2, zs)), dma((2, chunks)), dma((2, chunks, n_tp)), dma((2, chunks, n_tp)),
            dma((2, chunks)), dma((2, chunks, n_tp)), dma((2, chunks, n_tp)),
        ],
        compiler_params=pltpu.CompilerParams(collective_id=0, has_side_effects=True, vmem_limit_bytes=48 << 20),
        name="dispatch",
    )(x, y)


def hail(zs, n_tp, z, c, t):
    barrier = pltpu.get_barrier_semaphore()
    for k in range(1, zs):
        pl.semaphore_signal(barrier, inc=1, device_id=((z + k) % zs * 2 + c, t), device_id_type=MESH)
    for k in range(1, n_tp):
        pl.semaphore_signal(barrier, inc=1, device_id=(z * 2 + c, (t + k) % n_tp), device_id_type=MESH)
    pl.semaphore_signal(barrier, inc=1, device_id=(z * 2 + 1 - c, t), device_id_type=MESH)
    return lambda: pl.semaphore_wait(barrier, zs + n_tp - 1)


def lane_sums(square):
    folded = square[:, :128]
    for k in range(1, square.shape[1] // 128):
        folded = folded + square[:, k * 128:(k + 1) * 128]
    return jnp.sum(folded.T, axis=0, keepdims=True)


def return_kernel(
    zs, n_tp, part,
    gate_hbm, up_hbm, w_gate_hbm, w_up_hbm, x_hbm, hidden_hbm, y_hbm, scores,
    out_rows, out_scores, out_norms, out_down_norms, gate_out, up_out, down_out,
    gate_grad, up_grad, w_gate, w_up, x, hidden, y, gate_full, up_full, down_full, norms, folded,
    all_rows, other, other_scores, both, both_scores, pieces, score_pieces, norm_pieces, total, total_scores,
    passing, passed, pass_send, pass_recv, sum_send, sum_recv, load_sem, store_sem,
    core_send, core_recv, cs_send, cs_recv, tp_send, tp_recv, ts_send, ts_recv,
    tn_send, tn_recv, ep_send, ep_recv, es_send, es_recv,
):
    z, c, t = places()
    chunks = zs if zs <= 4 else 1
    span = zs // chunks
    cap = out_rows.shape[1]
    width, hid = w_gate.shape
    half = zs * cap
    everyone_in = hail(zs, n_tp, z, c, t)
    loads = []
    for i, (src, dst) in enumerate((
        (gate_hbm, gate_grad), (up_hbm, up_grad), (w_gate_hbm, w_gate), (w_up_hbm, w_up),
        (x_hbm, x), (hidden_hbm, hidden), (y_hbm, y),
    )):
        copy = pltpu.make_async_copy(src, dst, load_sem.at[i])
        copy.start()
        loads.append(copy)
    stores = []

    def store(i, src, dst):
        copy = pltpu.make_async_copy(src, dst, store_sem.at[i])
        copy.start()
        stores.append(copy)

    across = (((1,), (1,)), ((), ()))
    down = (((0,), (0,)), ((), ()))
    tile = min(256, width)

    def row_terms():
        @pl.loop(0, width // tile)
        def _(j):
            at = pl.ds(pl.multiple_of(j * tile, tile), tile)
            term = (
                lax.dot_general(gate_grad[...].reshape(2 * half, hid), w_gate[at, :], across, preferred_element_type=F32)
                + lax.dot_general(up_grad[...].reshape(2 * half, hid), w_up[at, :], across, preferred_element_type=F32)
            ).astype(BF16)
            all_rows[0, :, at] = term[:half]
            all_rows[1, :, at] = term[half:]

    sent = []
    if chunks == 1:
        order = [0]
    else:
        order = [(z + k) % zs for k in reversed(distances(zs))] + [z]
    mate = z * 2 + 1 - c

    def rows_of(q):
        if chunks == 1:
            return slice(None)
        return pl.ds(pl.multiple_of(q * cap, cap), cap)

    for copy in loads[:4]:
        copy.wait()
    row_terms()
    everyone_in()
    for q in order:
        sent.append(send(all_rows.at[1 - c, rows_of(q)], other.at[rows_of(q)], core_send.at[q], core_recv.at[q], mate, t))
    sent.append(send(scores.at[1 - c], other_scores, cs_send, cs_recv, mate, t))

    def cols(feat):
        return pl.ds(pl.multiple_of(feat * part, part), part)

    def reduce_core(q):
        at = rows_of(q)
        arrived(other.at[at], core_recv.at[q])
        both[at, :] = (all_rows[c, at, :].astype(F32) + other[at, :].astype(F32)).astype(BF16)
        if n_tp == 4:
            far_side = tp_peer(t, 3, n_tp)
            for s in (1, 2):
                sent.append(send(both.at[at, half_cols(far_side, s - 1)], passing.at[s - 1, at], pass_send.at[s - 1, q], pass_recv.at[s - 1, q], z * 2 + c, tp_peer(t, s, n_tp)))
            for s in (1, 2):
                feat = tp_peer(t, s, n_tp)
                sent.append(send(both.at[at, half_cols(feat, s - 1)], piece_half(s, at, s - 1), tp_send.at[s, q], tp_recv.at[s, q], z * 2 + c, feat))
        else:
            for s in reversed(range(1, n_tp)):
                feat = tp_peer(t, s, n_tp)
                sent.append(send(both.at[at, cols(feat)], pieces.at[s, at], tp_send.at[s, q], tp_recv.at[s, q], z * 2 + c, feat))

    def half_cols(feat, u):
        return pl.ds(pl.multiple_of(feat * part + u * (part // 2), part // 2), part // 2)

    def piece_half(s, at, u):
        return pieces.at[s, at, pl.ds(u * (part // 2), part // 2)]

    def pass_on(q):
        if n_tp == 4:
            at = rows_of(q)
            for s in (1, 2):
                u, turn = s - 1, 3 - s
                feat = tp_peer(t, turn, n_tp)
                arrived(passing.at[u, at], pass_recv.at[u, q])
                passed[u, at, :] = (passing[u, at, :].astype(F32) + both[at, half_cols(feat, u)].astype(F32)).astype(BF16)
                sent.append(send(passed.at[u, at], piece_half(turn, at, u), sum_send.at[turn, q], sum_recv.at[turn, q], z * 2 + c, feat))

    for q in order:
        reduce_core(q)
    arrived(other_scores, cs_recv)
    both_scores[...] = scores[c] + other_scores[...]
    for s in range(1, n_tp):
        sent.append(send(both_scores, score_pieces.at[s], ts_send.at[s], ts_recv.at[s], z * 2 + c, tp_peer(t, s, n_tp)))

    def reduce_tp(q):
        at = rows_of(q)
        if n_tp == 4:
            for s in (1, 2):
                arrived(piece_half(s, at, s - 1), tp_recv.at[s, q])
                arrived(piece_half(s, at, 2 - s), sum_recv.at[s, q])
        else:
            for s in reversed(range(1, n_tp)):
                arrived(pieces.at[s, at], tp_recv.at[s, q])
        for j in range(span):
            sub = at if chunks > 1 else slice(j * cap, (j + 1) * cap)
            acc = both[sub, cols(t)].astype(F32)
            for s in (1, 2) if n_tp == 4 else range(1, n_tp):
                acc = acc + pieces[s, sub, :].astype(F32)
            total[q * span + j] = acc.astype(BF16)

    def go_home(dest, k):
        sent.append(send(total.at[dest], out_rows.at[z], ep_send.at[k], ep_recv.at[k], dest * 2 + c, t))

    def input_tiles(first, last):
        @pl.loop(first * tile // g_tile, last * tile // g_tile)
        def _(j):
            at = pl.ds(pl.multiple_of(j * g_tile, g_tile), g_tile)
            columns = x[:, at].T
            for i, (grad, full) in enumerate(((gate_grad, gate_full), (up_grad, up_full))):
                term = jnp.dot(columns, grad[...].reshape(2 * half, hid), preferred_element_type=F32)
                full[at, :] = term.astype(BF16)
                norms[pl.ds(i, 1), at] = lane_sums(term * term)

    h_tile = min(256, hid)
    g_tile = min(512, width)
    wide = min(512, width)

    def down_tiles(i):
        at = slice(i * h_tile, (i + 1) * h_tile)
        folded[...] = jnp.zeros_like(folded)
        turned = hidden[:, at].T

        @pl.loop(0, width // wide)
        def _(j):
            lanes = pl.ds(pl.multiple_of(j * wide, wide), wide)
            term = jnp.dot(turned, y[:, lanes], preferred_element_type=F32)
            down_full[at, lanes] = term.astype(BF16)
            square = term * term
            acc = square[:, :128]
            for k in range(1, wide // 128):
                acc = acc + square[:, k * 128:(k + 1) * 128]
            folded[...] += acc

        out_down_norms[:, at] = jnp.sum(folded[...].T, axis=0, keepdims=True)

    away = list(reversed(distances(zs)))
    n_tiles = width // tile

    def phase_input(first, last):
        if first == 0:
            loads[4].wait()
        input_tiles(first, last)
        if last == n_tiles:
            store(0, gate_full, gate_out)
            store(1, up_full, up_out)
            for s in range(1, n_tp):
                sent.append(send(norms, norm_pieces.at[s], tn_send.at[s], tn_recv.at[s], z * 2 + c, tp_peer(t, s, n_tp)))

    def phase_down(first, last):
        if first == 0:
            loads[5].wait()
            loads[6].wait()
        for i in range(first, last):
            down_tiles(i)
        if last == hid // h_tile:
            store(2, down_full, down_out)

    h_count = hid // h_tile
    phases = [
        lambda: phase_input(0, n_tiles // 2),
        lambda: phase_input(n_tiles // 2, n_tiles),
        lambda: phase_down(0, h_count // 2) if h_count > 1 else None,
        lambda: phase_down(h_count // 2, h_count),
    ]
    if chunks < len(phases):
        for phase in phases:
            phase()
        phases = []
    pass_on(order[0])
    if chunks > 1:
        pass_on(order[1])
    for i in range(chunks):
        if i < len(phases):
            phases[i]()
        if i + 2 < chunks:
            pass_on(order[i + 2])
        reduce_tp(order[i])
        if chunks > 1:
            if i < len(away):
                go_home(order[i], away[i])
        else:
            for k in away:
                go_home((z + k) % zs, k)
        if i == 0:
            for s in range(1, n_tp):
                arrived(score_pieces.at[s], ts_recv.at[s])
            acc = both_scores[...]
            for s in range(1, n_tp):
                acc = acc + score_pieces[s]
            total_scores[...] = acc
            for k in away:
                dest = (z + k) % zs
                sent.append(send(total_scores.at[dest], out_scores.at[z], es_send.at[k], es_recv.at[k], dest * 2 + c, t))
            out_scores[z] = total_scores[z]
    out_rows[z] = total[z]
    acc = norms[...]
    for s in range(1, n_tp):
        arrived(norm_pieces.at[s], tn_recv.at[s])
        acc = acc + norm_pieces[s]
    out_norms[...] = acc
    for k in away:
        src = (z + zs - k) % zs
        arrived(out_scores.at[src], es_recv.at[k])
        arrived(out_rows.at[src], ep_recv.at[k])
    for copy in stores:
        copy.wait()
    for copy in sent:
        copy.wait_send()


def send_back(gate_grad, up_grad, w_gate, w_up, x, hidden, y, scores, zs, n_tp):
    rows, width = x.shape
    hid = hidden.shape[1]
    part, half = width // n_tp, rows // 2
    cap = half // zs
    chunks = zs if zs <= 4 else 1
    vm = pl.BlockSpec(memory_space=pltpu.VMEM)
    far = pl.BlockSpec(memory_space=pltpu.HBM)
    dma = pltpu.SemaphoreType.DMA
    line = scores.shape[2:]
    gradient = jax.ShapeDtypeStruct((width, hid), BF16)
    return pl.pallas_call(
        functools.partial(return_kernel, zs, n_tp, part),
        out_shape=(
            jax.ShapeDtypeStruct((zs, cap, part), BF16),
            jax.ShapeDtypeStruct((zs,) + line, F32),
            jax.ShapeDtypeStruct((2, width), F32),
            jax.ShapeDtypeStruct((1, hid), F32),
            gradient, gradient, jax.ShapeDtypeStruct((hid, width), BF16),
        ),
        in_specs=[far] * 7 + [vm],
        out_specs=(vm,) * 4 + (far,) * 3,
        scratch_shapes=[
            pltpu.VMEM((2, half, hid), BF16), pltpu.VMEM((2, half, hid), BF16),
            pltpu.VMEM((width, hid), BF16), pltpu.VMEM((width, hid), BF16),
            pltpu.VMEM((rows, width), BF16), pltpu.VMEM((rows, hid), BF16), pltpu.VMEM((rows, width), BF16),
            pltpu.VMEM((width, hid), BF16), pltpu.VMEM((width, hid), BF16), pltpu.VMEM((hid, width), BF16),
            pltpu.VMEM((2, width), F32), pltpu.VMEM((min(256, hid), 128), F32),
            pltpu.VMEM((2, half, width), BF16), pltpu.VMEM((half, width), BF16),
            pltpu.VMEM((zs,) + line, F32),
            pltpu.VMEM((half, width), BF16),
            pltpu.VMEM((zs,) + line, F32),
            pltpu.VMEM((n_tp, half, part), BF16),
            pltpu.VMEM((n_tp, zs) + line, F32),
            pltpu.VMEM((n_tp, 2, width), F32),
            pltpu.VMEM((zs, cap, part), BF16),
            pltpu.VMEM((zs,) + line, F32),
            pltpu.VMEM((2, half, part // 2), BF16), pltpu.VMEM((2, half, part // 2), BF16),
            dma((2, chunks)), dma((2, chunks)), dma((3, chunks)), dma((3, chunks)),
            dma((7,)), dma((3,)),
            dma((chunks,)), dma((chunks,)), dma, dma,
            dma((n_tp, chunks)), dma((n_tp, chunks)), dma((n_tp,)), dma((n_tp,)),
            dma((n_tp,)), dma((n_tp,)), dma((zs,)), dma((zs,)), dma((zs,)), dma((zs,)),
        ],
        compiler_params=pltpu.CompilerParams(collective_id=1, has_side_effects=True, vmem_limit_bytes=50 << 20),
        name="send_back",
    )(gate_grad.reshape(2, half, hid), up_grad.reshape(2, half, hid), w_gate, w_up, x, hidden, y, scores)


def on_device(tokens, routing, mixing, gate_matrix, up_matrix, down_matrix, upstream):
    experts = lax.axis_size("ep") // 2
    n_tp = lax.axis_size("tp")
    tok_rows, part = tokens.shape
    top = routing.shape[1]
    capacity = 5 * top * tok_rows // (4 * experts)
    slots = experts * capacity
    flat = routing.reshape(-1)
    choose = (flat[:, None] == jnp.arange(experts, dtype=jnp.int32)[None, :]).astype(BF16)
    pairs = top * tok_rows
    before = (jnp.arange(pairs)[:, None] > jnp.arange(pairs)[None, :]).astype(BF16)
    earlier = jnp.dot(before, choose, preferred_element_type=F32)
    target = flat * capacity + jnp.sum(earlier * choose.astype(F32), axis=1).astype(jnp.int32)
    spot = target.reshape(tok_rows, top)
    matches = (spot[:, :, None] == jnp.arange(slots, dtype=jnp.int32)[None, None, :])
    by_token = jnp.any(matches, axis=1).astype(BF16)
    scaled = (mixing[:, :, None] * upstream[:, None, :].astype(F32)).astype(BF16)
    rows_first = (((0,), (0,)), ((), ()))
    placed_x = lax.dot_general(by_token, tokens, rows_first, preferred_element_type=F32).astype(BF16)
    placed_y = lax.dot_general(
        matches.reshape(pairs, slots).astype(BF16), scaled.reshape(pairs, part), rows_first,
        preferred_element_type=F32,
    ).astype(BF16)
    x_all, y_all = dispatch(
        placed_x.reshape(experts, capacity, part), placed_y.reshape(experts, capacity, part), experts, n_tp
    )
    width = n_tp * part
    row_count = 2 * slots
    x = x_all.reshape(row_count, width)
    y = y_all.reshape(row_count, width)
    w_gate, w_up, w_down = gate_matrix[0], up_matrix[0], down_matrix[0]
    cols = (((1,), (1,)), ((), ()))
    gate_pre = jnp.dot(x, w_gate, preferred_element_type=F32)
    up_pre = jnp.dot(x, w_up, preferred_element_type=F32)
    back = lax.dot_general(y, w_down, cols, preferred_element_type=F32)
    sig = jax.nn.sigmoid(gate_pre)
    act = gate_pre * sig
    hidden = act * up_pre
    gate_grad = (back * up_pre * sig * (1.0 + gate_pre * (1.0 - sig))).astype(BF16)
    up_grad = (back * act).astype(BF16)
    scores = jnp.sum(hidden * back, axis=1)
    line = -(-capacity // 128) * 128
    scores = jnp.pad(scores.reshape(2, experts, 1, capacity), ((0, 0), (0, 0), (0, 0), (0, line - capacity)))
    back_rows, back_scores, norms_all, down_norms, gate_full, up_full, down_full = send_back(
        gate_grad, up_grad, w_gate, w_up, x, hidden.astype(BF16), y, scores, experts, n_tp
    )
    token_gradient = jnp.dot(
        by_token, back_rows.reshape(slots, part), preferred_element_type=F32
    ).astype(BF16)
    pair_scores = back_scores[:, 0, :capacity].reshape(slots)
    mixing_gradient = jnp.sum(jnp.where(matches, pair_scores[None, None, :], 0.0), axis=2) / mixing
    return (
        token_gradient,
        mixing_gradient,
        gate_full[None],
        up_full[None],
        down_full[None],
        norms_all[None],
        down_norms,
    )


def solution(mesh):
    placed = (
        P("ep", "tp"), P("ep", None), P("ep", None), P("ep", None, "tp"),
        P("ep", None, "tp"), P("ep", "tp", None), P("ep", "tp"),
    )
    return jax.shard_map(
        on_device,
        mesh=mesh,
        in_specs=placed,
        out_specs=(
            P("ep", "tp"), P("ep", None), P("ep", None, "tp"), P("ep", None, "tp"),
            P("ep", "tp", None), P("ep", None, None), P("ep", "tp"),
        ),
        check_vma=False,
    )
```

profile of v0, /device:TPU:0, one launch (start us, length us, event | category | flops | bytes accessed | tf_op | source)
XLA Modules:
  0.0 85.7 jit_solution(1214549930075671161)
XLA Ops:
  0.6 0.0 copy-start
  0.6 0.9 %copy.22 = s32[128,2]{1,0:T(8,128)S(1)} copy(s32[128,2]{0,1:T(2,128)} %param.8) | data formatting | bytes 2048 | tf_op args[1]
  1.6 0.1 eq.28
  1.7 0.2 fusion.4
  1.9 0.1 convert_element_type.47
  2.1 0.1 copy.23
  2.1 0.0 copy-start.7
  2.1 0.9 multiply_add_fusion
  3.0 0.9 %convert_element_type.49 = f32[128,512]{1,0:T(8,128)S(1)} convert(bf16[128,512]{1,0:T(8,128)(2,1)} %param.13) | non-fusion elementwise | flops 65536 | bytes 393216 | tf_op jit(solution)/shard_map/convert_element_type | solution.py:485
  4.0 1.0 %fusion.3 = bf16[320,512]{1,0:T(8,128)(2,1)S(1)} fusion(f32[128,512]{1,0:T(8,128)S(1)} %convert_element_type.49, f32[128,2]{0,1:T(2,128)} %param.9, s32[128,2]{0,1:T(2,128)S(1)} %multiply_add_fusion), kind=kOutput, calls=%fused_computation.8 | convolution fusion | flops 84393984 | bytes 591872 | tf_op jit(solution)/shard_map/dot_general | solution.py:488
  5.0 1.1 %convolution_convert_fusion = bf16[320,512]{1,0:T(8,128)(2,1)S(1)} fusion(pred[128,320]{0,1:T(8,128)(4,1)S(1)} %fusion.5, bf16[128,512]{1,0:T(8,128)(2,1)} %param.7), kind=kOutput, calls=%fused_computation.9 | convolution fusion | flops 42106880 | bytes 499712 | tf_op jit(solution)/shard_map/dot_general | solution.py:487
  6.1 32.4 %dispatch.1 = (bf16[2,4,80,2048]{3,2,1,0:T(8,128)(2,1)S(1)}, bf16[2,4,80,2048]{3,2,1,0:T(8,128)(2,1)S(1)}) custom-call(bf16[4,80,512]{2,1,0:T(8,128)(2,1)S(1)} %bitcast.39, bf16[4,80,512]{2,1,0:T(8,128)(2,1)S(1)} %bitcast.38), custom_call_target="tpu_custom_call" | custom-call | tf_op jit(solution)/shard_map/dispatch/pallas_call | solution.py:154
  38.5 0.0 copy-start.1
  38.5 0.0 copy-start.2
  38.6 0.0 copy-done.7
  38.6 0.0 copy-start.6
  38.6 1.5 %fusion.11 = f32[640,512]{1,0:T(8,128)S(1)} fusion(bf16[640,2048]{1,0:T(8,128)(2,1)S(1)} %bitcast.33, bf16[1,2048,512]{2,1,0:T(8,128)(2,1)S(1)} %copy-done.7), kind=kOutput, calls=%fused_computation.27 | convolution fusion | flops 1342177280 | bytes 6029312 | tf_op jit(solution)/shard_map/dot_general | solution.py:501
  40.1 0.0 copy-done.1
  40.1 1.6 %copy-done.6 = bf16[1,2048,512]{2,1,0:T(8,128)(2,1)S(1)} copy-done((bf16[1,2048,512]{2,1,0:T(8,128)(2,1)S(1)}, bf16[1,2048,512]{2,1,0:T(8,128)(2,1)}, u32[]{:S(2)}) %copy-start.6) | copy-done | bytes 2097176
  41.7 1.5 %fusion.13 = f32[640,512]{1,0:T(8,128)S(1)} fusion(bf16[640,2048]{1,0:T(8,128)(2,1)S(1)} %bitcast.34, bf16[1,2048,512]{2,1,0:T(8,128)(2,1)S(1)} %copy-done.6), kind=kOutput, calls=%fused_computation.29 | convolution fusion | flops 1342177280 | bytes 6029312 | tf_op jit(solution)/shard_map/dot_general | solution.py:502
  43.3 0.0 copy-done.2
  43.3 0.0 copy-done
  43.3 2.9 %multiply_reduce_fusion = (f32[640]{0:T(1024)S(1)}, bf16[640,512]{1,0:T(8,128)(2,1)S(1)}, bf16[640,512]{1,0:T(8,128)(2,1)S(1)}, bf16[640,512]{1,0:T(8,128)(2,1)}) fusion(f32[640,512]{1,0:T(8,128)S(1)} %fusion.13, f32[640,512]{1,0:T(8,128)S(1)} %fusion.11, bf16[640,2048]{1,0:T(8,128)(2,1)S(1)} %bitcast.36, bf16[1,512,2048]{2,1,0:T(8,128)(2,1)S(1)} %copy-done), kind=kOutput, calls=%fused_computation.2 | convolution fusion | flops 1347747200 | bytes 9308672 | tf_op jit(solution)/shard_map/dot_general | solution.py:503
  46.2 0.1 reshape.60
  46.3 0.0 copy-start.3
  46.3 1.1 %copy-done.3 = bf16[640,512]{1,0:T(8,128)(2,1)S(1)} copy-done((bf16[640,512]{1,0:T(8,128)(2,1)S(1)}, bf16[640,512]{1,0:T(8,128)(2,1)}, u32[]{:S(2)}) %copy-start.3) | copy-done | bytes 655384
  47.4 0.0 copy-start.8
  47.4 28.4 %send_back.1 = (bf16[4,80,512]{2,1,0:T(8,128)(2,1)S(1)}, f32[4,1,128]{2,1,0:T(1,128)S(1)}, f32[2,2048]{1,0:T(2,128)S(1)}, f32[1,512]{1,0:T(1,128)S(1)}, bf16[204...) custom-call(bf16[2,320,512]{2,1,0:T(8,128)(2,1)S(1)} %bitcast.40, ...), custom_call_target="tpu_custom_call" | custom-call | tf_op jit(solution)/shard_map/send_back/pallas_call | solution.py:431
  75.9 0.9 %convolution_convert_fusion.1 = bf16[128,512]{1,0:T(8,128)(2,1)} fusion(pred[128,320]{0,1:T(8,128)(4,1)S(1)} %fusion.5, bf16[320,512]{1,0:T(8,128)(2,1)S(1)} %bitcast.42), kind=kOutput, calls=%fused_computation.10 | convolution fusion | flops 42008576 | bytes 499712 | tf_op jit(solution)/shard_map/dot_general | solution.py:515
  76.8 0.1 broadcast_in_dim.32
  76.9 0.1 select_reduce_fusion
  77.0 0.0 copy-done.8
  77.0 0.6 div.7
  77.6 0.0 copy-start.5
  77.6 3.2 %copy.29 = bf16[1,2048,512]{2,1,0:T(8,128)(2,1)} copy(bf16[1,2048,512]{2,1,0:T(8,128)(2,1)} %bitcast.46) | data formatting | bytes 4194304
  80.8 0.0 copy-done.5
  80.8 0.0 copy-start.4
  80.8 1.3 %copy.30 = bf16[1,2048,512]{2,1,0:T(8,128)(2,1)} copy(bf16[1,2048,512]{2,1,0:T(8,128)(2,1)S(1)} %bitcast.45) | data formatting | bytes 4194304
  82.1 1.0 %copy-done.4 = bf16[512,2048]{1,0:T(8,128)(2,1)S(1)} copy-done((bf16[512,2048]{1,0:T(8,128)(2,1)S(1)}, bf16[512,2048]{1,0:T(8,128)(2,1)}, u32[]{:S(2)}) %copy-start.4) | copy-done | bytes 2097176
  83.2 1.3 %copy.31 = bf16[1,512,2048]{2,1,0:T(8,128)(2,1)} copy(bf16[1,512,2048]{2,1,0:T(8,128)(2,1)S(1)} %bitcast.44) | data formatting | bytes 4194304
  84.5 0.6 copy.32
  85.1 0.6 copy.33
  (4 shorter events, 0.1 us)
Async XLA Ops:
  0.6 42.7 %copy-start = (bf16[1,512,2048]{2,1,0:T(8,128)(2,1)S(1)}, bf16[1,512,2048]{2,1,0:T(8,128)(2,1)}, u32[]{:S(2)}) copy-start(bf16[1,512,2048]{2,1,0:T(8,128)(2,1)} %param.12) | copy-start | bytes 6291460
  2.1 36.4 %copy-start.7 = (bf16[1,2048,512]{2,1,0:T(8,128)(2,1)S(1)}, bf16[1,2048,512]{2,1,0:T(8,128)(2,1)}, u32[]{:S(2)}) copy-start(bf16[1,2048,512]{2,1,0:T(8,128)(2,1)} %param.10) | copy-start | bytes 6291460
  38.5 1.6 %copy-start.1 = (bf16[2,4,80,2048]{3,2,1,0:T(8,128)(2,1)}, bf16[2,4,80,2048]{3,2,1,0:T(8,128)(2,1)S(1)}, u32[]{:S(2)}) copy-start(bf16[2,4,80,2048]{3,2,1,0:T(8,128)(2,1)S(1)} %get-tuple-element.17) | copy-start | bytes 7864324
  38.5 4.7 %copy-start.2 = (bf16[2,4,80,2048]{3,2,1,0:T(8,128)(2,1)}, bf16[2,4,80,2048]{3,2,1,0:T(8,128)(2,1)S(1)}, u32[]{:S(2)}) copy-start(bf16[2,4,80,2048]{3,2,1,0:T(8,128)(2,1)S(1)} %get-tuple-element.16) | copy-start | bytes 7864324
  38.6 3.2 %copy-start.6 = (bf16[1,2048,512]{2,1,0:T(8,128)(2,1)S(1)}, bf16[1,2048,512]{2,1,0:T(8,128)(2,1)}, u32[]{:S(2)}) copy-start(bf16[1,2048,512]{2,1,0:T(8,128)(2,1)} %param.11) | copy-start | bytes 6291460
  46.3 1.1 %copy-start.3 = (bf16[640,512]{1,0:T(8,128)(2,1)S(1)}, bf16[640,512]{1,0:T(8,128)(2,1)}, u32[]{:S(2)}) copy-start(bf16[640,512]{1,0:T(8,128)(2,1)} %get-tuple-element.28) | copy-start | bytes 1966084
  47.4 29.6 %copy-start.8 = (f32[128,2]{0,1:T(2,128)S(1)}, f32[128,2]{0,1:T(2,128)}, u32[]{:S(2)}) copy-start(f32[128,2]{0,1:T(2,128)} %param.9) | copy-start | bytes 3076
  77.6 3.2 %copy-start.5 = (bf16[2048,512]{1,0:T(8,128)(2,1)S(1)}, bf16[2048,512]{1,0:T(8,128)(2,1)}, u32[]{:S(2)}) copy-start(bf16[2048,512]{1,0:T(8,128)(2,1)} %get-tuple-element.21) | copy-start | bytes 6291460
  80.8 2.3 %copy-start.4 = (bf16[512,2048]{1,0:T(8,128)(2,1)S(1)}, bf16[512,2048]{1,0:T(8,128)(2,1)}, u32[]{:S(2)}) copy-start(bf16[512,2048]{1,0:T(8,128)(2,1)} %get-tuple-element.22) | copy-start | bytes 6291460
where the time goes:
time: 86 us; the launch traced here: 85.7 us
  Pallas kernels  60.8 us (71%)
  local copies, waits for them, and re-layouts  12.2 us (14%)
  matrix products  9.27 us (11%)
  other arithmetic  2.52 us (3%)
    pallas_call x1, Pallas kernels, dispatch(): pl.pallas_call(functools.partial(dispatch_kernel, zs, n_tp, part), out_sh...  32.4 us
    pallas_call x1, Pallas kernels, send_back(): pl.pallas_call(functools.partial(return_kernel, zs, n_tp, part), out_shap...  28.4 us
    unnamed x24, local copies, waits for them, and re-layouts  11.7 us
    dot_general x1, matrix products, on_device(): back = lax.dot_general(y, w_down, cols, preferred_element_type=F32)  2.95 us

commit v1 on v0

--- a/solution.py
+++ b/solution.py
@@ -466,12 +466,470 @@
     )(gate_grad.reshape(2, half, hid), up_grad.reshape(2, half, hid), w_gate, w_up, x, hidden, y, scores)
 
 
+def fused_kernel(
+    zs, n_tp, part, cap, tok,
+    routing_hbm, mixing_hbm, tokens_hbm, upstream_hbm, w_gate_hbm, w_up_hbm, w_down_hbm,
+    tokens_out, mixing_out, norms_out, down_norms_out, gate_out, up_out, down_out,
+    out_tokens, out_mixing, out_norms, out_down_norms, gate_full, up_full, down_full,
+    routing, mixing, tokens, upstream, w_gate, w_up, w_down, gate_turned, up_turned, down_turned,
+    x_put, y_put, x_all, y_all, gate_grad, up_grad, hidden, targets,
+    all_rows, other, both, passing, passed, pieces, total, back_rows,
+    scores, other_scores, both_scores, score_pieces, total_scores, back_scores,
+    norms, norm_pieces,
+    folded, load_sem, store_sem, own_sem, ep_send, ep_recv, tp_send, tp_recv, fwd_send, core_send, core_recv,
+    swap_send, swap_recv, pass_send, pass_recv, half_send, half_recv, sum_send, sum_recv,
+    cs_send, cs_recv, ts_send, ts_recv, tn_send, tn_recv, home_send, home_recv, es_send, es_recv,
+):
+    z, c, t = places()
+    here, mate = z * 2 + c, z * 2 + 1 - c
+    peers = [tp_peer(t, s, n_tp) for s in range(n_tp)]
+    width, hid = w_gate.shape
+    rows = 2 * cap
+    everyone_in = hail(zs, n_tp, z, c, t)
+    loads = []
+    for i, (src, dst) in enumerate((
+        (routing_hbm, routing), (mixing_hbm, mixing), (tokens_hbm, tokens), (upstream_hbm, upstream),
+        (w_down_hbm, w_down), (w_gate_hbm, w_gate), (w_up_hbm, w_up),
+    )):
+        copy = pltpu.make_async_copy(src, dst, load_sem.at[i])
+        copy.start()
+        loads.append(copy)
+    across = (((1,), (1,)), ((), ()))
+    first = (((0,), (0,)), ((), ()))
+    stores = []
+
+    def store(i, src, dst):
+        copy = pltpu.make_async_copy(src, dst, store_sem.at[i])
+        copy.start()
+        stores.append(copy)
+
+    def push(src, dst, send_sem, recv_sem, ep, tp):
+        send(src, dst, send_sem, recv_sem, ep, tp)
+
+    def cols(feat):
+        return pl.ds(pl.multiple_of(feat * part, part), part)
+
+    def half_cols(feat, u):
+        return pl.ds(pl.multiple_of(feat * part + u * (part // 2), part // 2), part // 2)
+
+    lanes = -(-zs // 16) * 16
+    experts_at = lax.broadcasted_iota(jnp.int32, (lanes, tok), 0)
+    before = lax.broadcasted_iota(jnp.int32, (tok, tok), 0) < lax.broadcasted_iota(jnp.int32, (tok, tok), 1)
+    for copy in loads[:2]:
+        copy.wait()
+    picks = [routing[k:k + 1, :] == experts_at for k in range(routing.shape[0])]
+    chosen = sum(pick.astype(F32) for pick in picks)
+    earlier = jnp.dot(chosen.astype(BF16), before.astype(F32).astype(BF16), preferred_element_type=F32)
+    for k, pick in enumerate(picks):
+        place = jnp.sum(jnp.where(pick, earlier, 0.0), axis=0, keepdims=True)
+        targets[k:k + 1, :] = routing[k:k + 1, :] * cap + place.astype(jnp.int32)
+
+    def matches(e):
+        slots_at = lax.broadcasted_iota(jnp.int32, (cap, tok), 0) + e * cap
+        return [targets[k:k + 1, :] == slots_at for k in range(len(picks))]
+
+    for copy in loads[2:4]:
+        copy.wait()
+    for e in range(zs):
+        hits = matches(e)
+        pick = sum(hit.astype(F32) for hit in hits).astype(BF16)
+        weight = sum(jnp.where(hit, mixing[k:k + 1, :], 0.0) for k, hit in enumerate(hits))
+        x_put[e] = jnp.dot(pick, tokens[...], preferred_element_type=F32).astype(BF16)
+        placed = jnp.dot(pick, upstream[...], preferred_element_type=F32)
+        y_put[e] = (placed * jnp.sum(weight, axis=1, keepdims=True)).astype(BF16)
+    scores[...] = jnp.zeros_like(scores)
+    everyone_in()
+
+    outer = (z - 1) * (z - 2) // 2
+    order = [z, z + 1 - 2 * (z % 2), 2 - z // 2, 3 - 3 * (z // 2)]
+    lands = [0, 1, 2 + outer, 2 + outer]
+    puts, alls = (x_put, y_put), (x_all, y_all)
+
+    def block(a, i, core, feat):
+        return alls[a].at[i, core, :, cols(feat)]
+
+    owns = []
+    for a in range(2):
+        copy = pltpu.make_async_copy(puts[a].at[z], block(a, 0, c, t), own_sem.at[a])
+        copy.start()
+        owns.append(copy)
+
+    def over(i):
+        return [
+            pltpu.make_async_remote_copy(
+                src_ref=puts[a].at[order[i]], dst_ref=block(a, lands[i], c, t), send_sem=ep_send.at[a],
+                recv_sem=ep_recv.at[a, lands[i]], device_id=(order[i] * 2 + c, t), device_id_type=MESH,
+            )
+            for a in range(2)
+        ]
+
+    def cross(i):
+        for copy in over(i):
+            copy.start()
+
+    def to_core(a, i, feat, src=None):
+        ref = block(a, i, c, feat)
+        push(ref if src is None else src, ref, core_send.at[a], core_recv.at[a, i, feat], mate, t)
+
+    def spread(i):
+        refs = [block(a, i, c, t) for a in range(2)]
+        srcs = refs if i else [puts[a].at[z] for a in range(2)]
+        if i:
+            for a in range(2):
+                arrived(refs[a], ep_recv.at[a, i])
+        for a, s in ((0, 1), (1, 2), (1, 1), (0, 2)):
+            push(srcs[a], refs[a], tp_send.at[a], tp_recv.at[a, i, t], here, peers[s])
+        for a in range(2):
+            to_core(a, i, t, srcs[a])
+
+    def relay(i):
+        for a, s in ((0, 1), (1, 2)):
+            ref = block(a, i, c, peers[s])
+            arrived(ref, tp_recv.at[a, i, peers[s]])
+            push(ref, ref, fwd_send.at[a], tp_recv.at[a, i, peers[s]], here, peers[3 - s])
+            to_core(a, i, peers[s])
+
+    def finish(i):
+        for a, s in ((1, 1), (0, 2), (0, 3), (1, 3)):
+            arrived(block(a, i, c, peers[s]), tp_recv.at[a, i, peers[s]])
+            to_core(a, i, peers[s])
+
+    square = min(256, hid)
+    eye = (
+        lax.broadcasted_iota(jnp.int32, (square, square), 0) == lax.broadcasted_iota(jnp.int32, (square, square), 1)
+    ).astype(F32).astype(BF16)
+
+    def turn_down():
+        loads[4].wait()
+
+        @pl.loop(0, width // square, unroll=4)
+        def _(j):
+            at = pl.ds(pl.multiple_of(j * square, square), square)
+            down_turned[at, :] = lax.dot_general(eye, w_down[:, at], across, preferred_element_type=F32).astype(BF16)
+
+    def turn_in(a):
+        loads[5 + a].wait()
+        src, dst = ((w_gate, gate_turned), (w_up, up_turned))[a]
+
+        @pl.loop(0, width // square, unroll=4)
+        def _(j):
+            at = pl.ds(pl.multiple_of(j * square, square), square)
+            for h in range(hid // square):
+                lines = slice(h * square, (h + 1) * square)
+                dst[lines, at] = lax.dot_general(eye, src[at, lines], across, preferred_element_type=F32).astype(BF16)
+
+    h_tile = min(256, hid)
+
+    def forward(i):
+        if i == 0:
+            for copy in owns:
+                copy.wait()
+        for a in range(2):
+            for feat in peers:
+                arrived(block(a, i, 1 - c, feat), core_recv.at[a, i, feat])
+        for j in range(hid // h_tile):
+            at = slice(j * h_tile, (j + 1) * h_tile)
+            gate_pre = jnp.dot(x_all[i].reshape(rows, width), w_gate[:, at], preferred_element_type=F32)
+            up_pre = jnp.dot(x_all[i].reshape(rows, width), w_up[:, at], preferred_element_type=F32)
+            back = jnp.dot(y_all[i].reshape(rows, width), down_turned[:, at], preferred_element_type=F32)
+            sig = jax.nn.sigmoid(gate_pre)
+            act = gate_pre * sig
+            low = act * up_pre
+            gate_grad[i, :, :, at] = (back * up_pre * sig * (1.0 + gate_pre * (1.0 - sig))).astype(BF16).reshape(2, cap, h_tile)
+            up_grad[i, :, :, at] = (back * act).astype(BF16).reshape(2, cap, h_tile)
+            hidden[i, :, :, at] = low.astype(BF16).reshape(2, cap, h_tile)
+            terms = low * back
+            for core in range(2):
+                scores[core, i, :, :cap] += lane_sums(terms[core * cap:(core + 1) * cap])
+
+    def row_terms(i):
+        for s in (3, 1, 2, 0):
+            at = cols(peers[s])
+            term = (
+                jnp.dot(gate_grad[i].reshape(rows, hid), gate_turned[:, at], preferred_element_type=F32)
+                + jnp.dot(up_grad[i].reshape(rows, hid), up_turned[:, at], preferred_element_type=F32)
+            ).astype(BF16)
+            all_rows[i, :, :, at] = term.reshape(2, cap, part)
+            push(all_rows.at[i, 1 - c, :, at], other.at[i, :, at], swap_send, swap_recv.at[i, s], mate, t)
+
+    def piece_half(s, i, u):
+        return pieces.at[s - 1, i, :, pl.ds(u * (part // 2), part // 2)]
+
+    def reduce_core(i):
+        for s in (3, 1, 2, 0):
+            at = cols(peers[s])
+            arrived(other.at[i, :, at], swap_recv.at[i, s])
+            both[i, :, at] = (all_rows[i, c, :, at].astype(F32) + other[i, :, at].astype(F32)).astype(BF16)
+            if s == 3:
+                for u in range(2):
+                    push(both.at[i, :, half_cols(peers[3], u)], passing.at[u, i], pass_send, pass_recv.at[u, i], here, peers[u + 1])
+            elif s:
+                u = s - 1
+                push(both.at[i, :, half_cols(peers[s], u)], piece_half(s, i, u), half_send, half_recv.at[u, i], here, peers[s])
+
+    def pass_on(i):
+        for u in range(2):
+            turn = 2 - u
+            arrived(passing.at[u, i], pass_recv.at[u, i])
+            passed[u, i] = (passing[u, i].astype(F32) + both[i, :, half_cols(peers[turn], u)].astype(F32)).astype(BF16)
+            push(passed.at[u, i], piece_half(turn, i, u), sum_send, sum_recv.at[turn - 1, i], here, peers[turn])
+
+    def reduce_tp(i):
+        for s in (1, 2):
+            arrived(piece_half(s, i, s - 1), half_recv.at[s - 1, i])
+            arrived(piece_half(s, i, 2 - s), sum_recv.at[s - 1, i])
+        acc = both[i, :, cols(t)].astype(F32) + pieces[0, i].astype(F32) + pieces[1, i].astype(F32)
+        if i == 0:
+            back_rows[z] = acc.astype(BF16)
+        else:
+            total[i] = acc.astype(BF16)
+            push(total.at[i], back_rows.at[z], home_send, home_recv.at[z], order[i] * 2 + c, t)
+
+    g_tile = min(512, width)
+
+    def input_tiles(begin, end):
+        @pl.loop(begin, end)
+        def _(j):
+            at = pl.ds(pl.multiple_of(j * g_tile, g_tile), g_tile)
+            columns = x_all[:, :, :, at].reshape(zs * rows, g_tile).T
+            for i, (grad, full) in enumerate(((gate_grad, gate_full), (up_grad, up_full))):
+                term = jnp.dot(columns, grad[...].reshape(zs * rows, hid), preferred_element_type=F32)
+                full[at, :] = term.astype(BF16)
+                norms[pl.ds(i, 1), at] = lane_sums(term * term)
+
+        if end == n_in:
+            store(4, gate_full, gate_out)
+            store(5, up_full, up_out)
+
+    def down_tiles():
+        turned = hidden[...].reshape(zs * rows, hid).T
+        folded[...] = jnp.zeros_like(folded)
+
+        @pl.loop(0, width // g_tile)
+        def _(j):
+            at = pl.ds(pl.multiple_of(j * g_tile, g_tile), g_tile)
+            term = jnp.dot(turned, y_all[:, :, :, at].reshape(zs * rows, g_tile), preferred_element_type=F32)
+            down_full[:, at] = term.astype(BF16)
+            term = term * term
+            acc = term[:, :128]
+            for k in range(1, g_tile // 128):
+                acc = acc + term[:, k * 128:(k + 1) * 128]
+            folded[...] += acc
+
+        store(6, down_full, down_out)
+        out_down_norms[...] = jnp.sum(folded[...].T, axis=0, keepdims=True)
+        store(3, out_down_norms, down_norms_out)
+
+    def send_norms():
+        for s in range(1, n_tp):
+            push(norms, norm_pieces.at[s], tn_send, tn_recv.at[s], here, peers[s])
+
+    def swap_scores():
+        push(scores.at[1 - c], other_scores, cs_send, cs_recv, mate, t)
+
+    def spread_scores():
+        arrived(other_scores, cs_recv)
+        both_scores[...] = scores[c] + other_scores[...]
+        for s in range(1, n_tp):
+            push(both_scores, score_pieces.at[s], ts_send, ts_recv.at[s], here, peers[s])
+
+    def home_scores():
+        acc = both_scores[...]
+        for s in range(1, n_tp):
+            arrived(score_pieces.at[s], ts_recv.at[s])
+            acc = acc + score_pieces[s]
+        total_scores[...] = acc
+        for i in range(1, zs):
+            push(total_scores.at[i], back_scores.at[z], es_send, es_recv.at[z], order[i] * 2 + c, t)
+        back_scores[z] = total_scores[0]
+
+    def close_norms():
+        acc = norms[...]
+        for s in range(1, n_tp):
+            arrived(norm_pieces.at[s], tn_recv.at[s])
+            acc = acc + norm_pieces[s]
+        out_norms[...] = acc
+        store(2, out_norms, norms_out)
+
+    def close_scores():
+        for q in order[1:]:
+            arrived(back_scores.at[q], es_recv.at[q])
+        for k in range(len(picks)):
+            found = jnp.zeros((1, tok), F32)
+            for e in range(zs):
+                column = jnp.broadcast_to(back_scores[e], (8, back_scores.shape[2])).T[:cap, :1]
+                found = found + jnp.sum(jnp.where(matches(e)[k], column, 0.0), axis=0, keepdims=True)
+            out_mixing[k:k + 1, :] = found / mixing[k:k + 1, :]
+        store(1, out_mixing, mixing_out)
+
+    def close_tokens():
+        for q in order[1:]:
+            arrived(back_rows.at[q], home_recv.at[q])
+        acc = jnp.zeros((tok, part), F32)
+        for e in range(zs):
+            pick = sum(hit.astype(F32) for hit in matches(e)).astype(BF16)
+            acc = acc + lax.dot_general(pick, back_rows[e], first, preferred_element_type=F32)
+        out_tokens[...] = acc.astype(BF16)
+        store(0, out_tokens, tokens_out)
+
+    n_in = width // g_tile
+    cross(1)
+
+    @pl.when(outer == 0)
+    def _():
+        cross(3)
+        cross(2)
+
+    spread(0)
+    turn_down()
+    relay(0)
+    turn_in(0)
+    spread(1)
+    turn_in(1)
+    finish(0)
+
+    @pl.when(outer == 1)
+    def _():
+        cross(2)
+        cross(3)
+
+    relay(1)
+    forward(0)
+    spread(2)
+    row_terms(0)
+    finish(1)
+    forward(1)
+    relay(2)
+    spread(3)
+    row_terms(1)
+    finish(2)
+    relay(3)
+    reduce_core(0)
+    reduce_core(1)
+    forward(2)
+    row_terms(2)
+    finish(3)
+    pass_on(0)
+    forward(3)
+    swap_scores()
+    pass_on(1)
+    reduce_core(2)
+    row_terms(3)
+    spread_scores()
+    pass_on(2)
+    reduce_core(3)
+    reduce_tp(0)
+    reduce_tp(1)
+    input_tiles(0, n_in // 2)
+    pass_on(3)
+    home_scores()
+    reduce_tp(2)
+    input_tiles(n_in // 2, n_in)
+    send_norms()
+    reduce_tp(3)
+    down_tiles()
+    close_norms()
+    close_scores()
+    close_tokens()
+    for copy in stores:
+        copy.wait()
+    for a in range(2):
+        arrived(puts[a].at[pl.ds(0, zs - 1)], ep_send.at[a])
+        arrived(alls[a].at[:, 0], core_send.at[a])
+        arrived(alls[a].at[:, 0, :, pl.ds(0, 2 * part)], tp_send.at[a])
+        arrived(alls[a].at[:, 0, :, pl.ds(0, part)], fwd_send.at[a])
+    arrived(other, swap_send)
+    for sem in (pass_send, half_send, sum_send):
+        arrived(passing, sem)
+    arrived(total.at[pl.ds(0, zs - 1)], home_send)
+    arrived(other_scores, cs_send)
+    arrived(score_pieces.at[pl.ds(0, n_tp - 1)], ts_send)
+    arrived(norm_pieces.at[pl.ds(0, n_tp - 1)], tn_send)
+    arrived(total_scores.at[pl.ds(0, zs - 1)], es_send)
+
+
+def settle_kernel(*refs):
+    count = len(refs) // 2
+    sem = refs[-1]
+    copies = [pltpu.make_async_copy(refs[i], refs[count + i], sem.at[i]) for i in range(count)]
+    for copy in copies:
+        copy.start()
+    for copy in copies:
+        copy.wait()
+
+
+def settle(arrays):
+    far = pl.BlockSpec(memory_space=pltpu.HBM)
+    vm = pl.BlockSpec(memory_space=pltpu.VMEM)
+    return pl.pallas_call(
+        settle_kernel,
+        out_shape=tuple(jax.ShapeDtypeStruct(a.shape, a.dtype) for a in arrays),
+        in_specs=[vm] * len(arrays),
+        out_specs=(far,) * len(arrays),
+        scratch_shapes=[pltpu.SemaphoreType.DMA((len(arrays),))],
+        compiler_params=pltpu.CompilerParams(vmem_limit_bytes=2 << 20),
+        name="settle",
+    )(*[pltpu.with_memory_space_constraint(a, pltpu.VMEM) for a in arrays])
+
+
+def fused(routing, mixing, tokens, upstream, w_gate, w_up, w_down, zs, n_tp, cap):
+    top, tok = routing.shape
+    part = tokens.shape[1]
+    width, hid = w_gate.shape
+    anywhere = pl.BlockSpec(memory_space=pl.ANY)
+    far = pl.BlockSpec(memory_space=pltpu.HBM)
+    dma = pltpu.SemaphoreType.DMA
+    line = -(-cap // 128) * 128
+
+    def room(*shape, kind=BF16):
+        return pltpu.VMEM(shape, kind)
+
+    return pl.pallas_call(
+        functools.partial(fused_kernel, zs, n_tp, part, cap, tok),
+        out_shape=(
+            room(tok, part), room(top, tok, kind=F32), room(2, width, kind=F32), room(1, hid, kind=F32),
+            room(width, hid), room(width, hid), room(hid, width),
+        ),
+        in_specs=[far] * 7,
+        out_specs=(anywhere,) * 7,
+        scratch_shapes=[
+            room(tok, part), room(top, tok, kind=F32), room(2, width, kind=F32), room(1, hid, kind=F32),
+            room(width, hid), room(width, hid), room(hid, width),
+            room(top, tok, kind=jnp.int32), room(top, tok, kind=F32), room(tok, part), room(tok, part),
+            room(width, hid), room(width, hid), room(hid, width), room(hid, width), room(hid, width), room(width, hid),
+            room(zs, cap, part), room(zs, cap, part), room(zs, 2, cap, width), room(zs, 2, cap, width),
+            room(zs, 2, cap, hid), room(zs, 2, cap, hid), room(zs, 2, cap, hid), room(top, tok, kind=jnp.int32),
+            room(zs, 2, cap, width), room(zs, cap, width), room(zs, cap, width),
+            room(2, zs, cap, part // 2), room(2, zs, cap, part // 2), room(2, zs, cap, part),
+            room(zs, cap, part), room(zs, cap, part),
+            room(2, zs, 1, line, kind=F32), room(zs, 1, line, kind=F32), room(zs, 1, line, kind=F32),
+            room(n_tp, zs, 1, line, kind=F32), room(zs, 1, line, kind=F32), room(zs, 1, line, kind=F32),
+            room(2, width, kind=F32), room(n_tp, 2, width, kind=F32), room(hid, 128, kind=F32),
+            dma((7,)), dma((7,)), dma((2,)), dma((2,)), dma((2, zs)), dma((2,)), dma((2, zs, n_tp)),
+            dma((2,)), dma((2,)), dma((2, zs, n_tp)),
+            dma, dma((zs, n_tp)), dma, dma((2, zs)), dma, dma((2, zs)), dma, dma((2, zs)),
+            dma, dma, dma, dma((n_tp,)), dma, dma((n_tp,)), dma, dma((zs,)), dma, dma((zs,)),
+        ],
+        compiler_params=pltpu.CompilerParams(collective_id=2, has_side_effects=True, vmem_limit_bytes=50 << 20),
+        name="fused",
+    )(*[pltpu.with_memory_space_constraint(a, pltpu.HBM) for a in (routing, mixing, tokens, upstream, w_gate, w_up, w_down)])
+
+
 def on_device(tokens, routing, mixing, gate_matrix, up_matrix, down_matrix, upstream):
     experts = lax.axis_size("ep") // 2
     n_tp = lax.axis_size("tp")
     tok_rows, part = tokens.shape
     top = routing.shape[1]
     capacity = 5 * top * tok_rows // (4 * experts)
+    if experts == 4 and n_tp == 4 and capacity % 16 == 0 and capacity <= 128:
+        results = fused(
+            routing.T, mixing.T, tokens, upstream, gate_matrix[0], up_matrix[0], down_matrix[0],
+            experts, n_tp, capacity,
+        )
+        grads, mixing_grad, norms_all, down_norms, gate_full, up_full, down_full = settle(results)
+        return (
+            grads, mixing_grad.T, gate_full[None], up_full[None], down_full[None], norms_all[None], down_norms,
+        )
     slots = experts * capacity
     flat = routing.reshape(-1)
     choose = (flat[:, None] == jnp.arange(experts, dtype=jnp.int32)[None, :]).astype(BF16)

time: 86 us -> 56.9 us (0.66)
  local copies, waits for them, and re-layouts: 12.2 us -> 0 us
  matrix products: 9.27 us -> 0 us
  Pallas kernels: 60.8 us -> 56.1 us
  other arithmetic: 2.52 us -> 0 us
    unnamed x24 -> x0, local copies, waits for them, and re-layouts: 11.7 us -> none
    dot_general x7 -> x0, matrix products: 9.27 us -> none  [the longest x1 2.95 us: on_device(): back = lax.dot_general(y, w_down, cols, preferred_element_type=F32)]
    pallas_call x2, Pallas kernels: 60.8 us -> 56.1 us  [the longest x1 53.3 us: fused(): pl.pallas_call(functools.partial(fused_kernel, zs, n_tp, part, cap, tok),...]
    convert_element_type x2 -> x0, other arithmetic: 0.93 us -> none  [the longest x1 0.93 us: on_device(): upstream[:, None, :].astype(F32)]
where the time goes in v1:
time: 56.9 us; the launch traced here: 56.7 us
  Pallas kernels  56.1 us (99%)
  between operations  0.64 us (1%)
    pallas_call x1, Pallas kernels, fused(): pl.pallas_call(functools.partial(fused_kernel, zs, n_tp, part, cap, tok),...  53.3 us
    pallas_call x1, Pallas kernels, settle(): pl.pallas_call(settle_kernel, out_shape=tuple((jax.ShapeDtypeStruct(a.sha...  2.82 us

profile of v1, /device:TPU:0, one launch (start us, length us, event | category | flops | bytes accessed | tf_op | source)
XLA Modules:
  0.0 56.7 jit_solution(6703280322773533238)
XLA Ops:
  0.6 53.3 %fused.1 = (bf16[128,512]{1,0:T(8,128)(2,1)S(1)}, f32[2,128]{1,0:T(2,128)S(1)}, f32[2,2048]{1,0:T(2,128)S(1)}, f32[1,512]{1,0:T(1,128)S(1)}, bf16[2048,512]{1,0:...) custom-call(s32[2,128]{1,0:T(2,128)} %bitcast.13, f32[2,128]{1,0:T(2,128)} %bitcast.14, ...), custom_call_target="tpu_custom_call" | custom-call | tf_op jit(solution)/shard_map/fused/pallas_call | solution.py:887
  53.9 2.8 %settle.1 = (bf16[128,512]{1,0:T(8,128)(2,1)}, f32[2,128]{1,0:T(2,128)}, f32[2,2048]{1,0:T(2,128)}, f32[1,512]{1,0:T(1,128)}, bf16[2048,512]{1,0:T(8,128)(2,1)},...) custom-call(bf16[128,512]{1,0:T(8,128)(2,1)S(1)} %get-tuple-element.21.refs_0_, ...), custom_call_target="tpu_custom_call" | custom-call | tf_op jit(solution)/shard_map/settle/pallas_call | solution.py:864

commit v2 on v1

--- a/solution.py
+++ b/solution.py
@@ -469,15 +469,14 @@
 def fused_kernel(
     zs, n_tp, part, cap, tok,
     routing_hbm, mixing_hbm, tokens_hbm, upstream_hbm, w_gate_hbm, w_up_hbm, w_down_hbm,
-    tokens_out, mixing_out, norms_out, down_norms_out, gate_out, up_out, down_out,
     out_tokens, out_mixing, out_norms, out_down_norms, gate_full, up_full, down_full,
     routing, mixing, tokens, upstream, w_gate, w_up, w_down, gate_turned, up_turned, down_turned,
     x_put, y_put, x_all, y_all, gate_grad, up_grad, hidden, targets,
     all_rows, other, both, passing, passed, pieces, total, back_rows,
     scores, other_scores, both_scores, score_pieces, total_scores, back_scores,
     norms, norm_pieces,
-    folded, load_sem, store_sem, own_sem, ep_send, ep_recv, tp_send, tp_recv, fwd_send, core_send, core_recv,
-    swap_send, swap_recv, pass_send, pass_recv, half_send, half_recv, sum_send, sum_recv,
+    folded, hidden_turned, load_sem, own_sem, ep_send, ep_recv, tp_send, tp_recv, fwd_send, core_send, core_recv,
+    swap_send, swap_recv, ring_send, pass_recv, sum_recv,
     cs_send, cs_recv, ts_send, ts_recv, tn_send, tn_recv, home_send, home_recv, es_send, es_recv,
 ):
     z, c, t = places()
@@ -485,7 +484,6 @@
     peers = [tp_peer(t, s, n_tp) for s in range(n_tp)]
     width, hid = w_gate.shape
     rows = 2 * cap
-    everyone_in = hail(zs, n_tp, z, c, t)
     loads = []
     for i, (src, dst) in enumerate((
         (routing_hbm, routing), (mixing_hbm, mixing), (tokens_hbm, tokens), (upstream_hbm, upstream),
@@ -494,15 +492,9 @@
         copy = pltpu.make_async_copy(src, dst, load_sem.at[i])
         copy.start()
         loads.append(copy)
+    everyone_in = hail(zs, n_tp, z, c, t)
     across = (((1,), (1,)), ((), ()))
     first = (((0,), (0,)), ((), ()))
-    stores = []
-
-    def store(i, src, dst):
-        copy = pltpu.make_async_copy(src, dst, store_sem.at[i])
-        copy.start()
-        stores.append(copy)
-
     def push(src, dst, send_sem, recv_sem, ep, tp):
         send(src, dst, send_sem, recv_sem, ep, tp)
 
@@ -541,23 +533,24 @@
     everyone_in()
 
     outer = (z - 1) * (z - 2) // 2
-    order = [z, z + 1 - 2 * (z % 2), 2 - z // 2, 3 - 3 * (z // 2)]
-    lands = [0, 1, 2 + outer, 2 + outer]
+    order = [z, 1 + z % 2, 3 - 3 * (z // 2), (2 + 3 * z) % 5]
+    lands = [0, 1 + 2 * outer, 3 - outer, 1 + outer]
     puts, alls = (x_put, y_put), (x_all, y_all)
 
     def block(a, i, core, feat):
         return alls[a].at[i, core, :, cols(feat)]
 
-    owns = []
+    def slab(a, i, feat, u):
+        return alls[a].at[i, c, :, half_cols(feat, u)]
+
     for a in range(2):
-        copy = pltpu.make_async_copy(puts[a].at[z], block(a, 0, c, t), own_sem.at[a])
+        copy = pltpu.make_async_copy(puts[a].at[z], block(a, 0, c, t), own_sem)
         copy.start()
-        owns.append(copy)
 
     def over(i):
         return [
             pltpu.make_async_remote_copy(
-                src_ref=puts[a].at[order[i]], dst_ref=block(a, lands[i], c, t), send_sem=ep_send.at[a],
+                src_ref=puts[a].at[order[i]], dst_ref=block(a, lands[i], c, t), send_sem=ep_send,
                 recv_sem=ep_recv.at[a, lands[i]], device_id=(order[i] * 2 + c, t), device_id_type=MESH,
             )
             for a in range(2)
@@ -569,30 +562,57 @@
 
     def to_core(a, i, feat, src=None):
         ref = block(a, i, c, feat)
-        push(ref if src is None else src, ref, core_send.at[a], core_recv.at[a, i, feat], mate, t)
-
-    def spread(i):
-        refs = [block(a, i, c, t) for a in range(2)]
-        srcs = refs if i else [puts[a].at[z] for a in range(2)]
-        if i:
+        push(ref if src is None else src, ref, core_send, core_recv.at[i], mate, t)
+
+    def spread(i, apart=False):
+        halves = [pl.ds(u * (part // 2), part // 2) for u in range(2)]
+
+        def land(a):
+            if i:
+                arrived(block(a, i, c, t), ep_recv.at[a, i])
+
+        def near(a):
+            for u in range(2):
+                ref = slab(a, i, t, u)
+                push(ref if i else puts[a].at[z, :, halves[u]], ref, tp_send, tp_recv.at[i, 2 * a + u], here, peers[1 + a])
+
+        def other_way(a):
+            ref = block(a, i, c, t)
+            push(ref if i else puts[a].at[z], ref, tp_send, tp_recv.at[i, 4], here, peers[2 - a])
+
+        def over_core(a):
+            to_core(a, i, t, None if i else puts[a].at[z])
+
+        if apart:
             for a in range(2):
-                arrived(refs[a], ep_recv.at[a, i])
-        for a, s in ((0, 1), (1, 2), (1, 1), (0, 2)):
-            push(srcs[a], refs[a], tp_send.at[a], tp_recv.at[a, i, t], here, peers[s])
+                land(a)
+                near(a)
+                other_way(a)
+                over_core(a)
+        else:
+            for step in (land, near, other_way, over_core):
+                for a in range(2):
+                    step(a)
+
+    def relay(i):
+        for u in range(2):
+            for a in range(2):
+                ref = slab(a, i, peers[1 + a], u)
+                arrived(ref, tp_recv.at[i, 2 * a + u])
+                push(ref, ref, fwd_send, tp_recv.at[i, 5], here, peers[2 - a])
         for a in range(2):
-            to_core(a, i, t, srcs[a])
-
-    def relay(i):
-        for a, s in ((0, 1), (1, 2)):
-            ref = block(a, i, c, peers[s])
-            arrived(ref, tp_recv.at[a, i, peers[s]])
-            push(ref, ref, fwd_send.at[a], tp_recv.at[a, i, peers[s]], here, peers[3 - s])
-            to_core(a, i, peers[s])
+            to_core(a, i, peers[1 + a])
+
+    def pair_of(i):
+        return x_all.at[i, :, :, pl.ds(0, part)]
 
     def finish(i):
-        for a, s in ((1, 1), (0, 2), (0, 3), (1, 3)):
-            arrived(block(a, i, c, peers[s]), tp_recv.at[a, i, peers[s]])
-            to_core(a, i, peers[s])
+        arrived(pair_of(i), tp_recv.at[i, 4])
+        for a in range(2):
+            to_core(a, i, peers[2 - a])
+        arrived(pair_of(i), tp_recv.at[i, 5])
+        for a in range(2):
+            to_core(a, i, peers[3])
 
     square = min(256, hid)
     eye = (
@@ -622,11 +642,8 @@
 
     def forward(i):
         if i == 0:
-            for copy in owns:
-                copy.wait()
-        for a in range(2):
-            for feat in peers:
-                arrived(block(a, i, 1 - c, feat), core_recv.at[a, i, feat])
+            arrived(pair_of(0), own_sem)
+        arrived(x_all.at[i], core_recv.at[i])
         for j in range(hid // h_tile):
             at = slice(j * h_tile, (j + 1) * h_tile)
             gate_pre = jnp.dot(x_all[i].reshape(rows, width), w_gate[:, at], preferred_element_type=F32)
@@ -642,15 +659,15 @@
             for core in range(2):
                 scores[core, i, :, :cap] += lane_sums(terms[core * cap:(core + 1) * cap])
 
-    def row_terms(i):
-        for s in (3, 1, 2, 0):
+    def row_terms(i, steps=(3, 1, 2, 0)):
+        for s in steps:
             at = cols(peers[s])
             term = (
                 jnp.dot(gate_grad[i].reshape(rows, hid), gate_turned[:, at], preferred_element_type=F32)
                 + jnp.dot(up_grad[i].reshape(rows, hid), up_turned[:, at], preferred_element_type=F32)
             ).astype(BF16)
             all_rows[i, :, :, at] = term.reshape(2, cap, part)
-            push(all_rows.at[i, 1 - c, :, at], other.at[i, :, at], swap_send, swap_recv.at[i, s], mate, t)
+            push(all_rows.at[i, 1 - c, :, at], other.at[i, :, at], swap_send, swap_recv.at[i, 0 if s == 3 else 1], mate, t)
 
     def piece_half(s, i, u):
         return pieces.at[s - 1, i, :, pl.ds(u * (part // 2), part // 2)]
@@ -658,26 +675,27 @@
     def reduce_core(i):
         for s in (3, 1, 2, 0):
             at = cols(peers[s])
-            arrived(other.at[i, :, at], swap_recv.at[i, s])
+            if s == 3:
+                arrived(other.at[i, :, at], swap_recv.at[i, 0])
+            elif s == 1:
+                arrived(other.at[i, :, pl.ds(0, (n_tp - 1) * part)], swap_recv.at[i, 1])
             both[i, :, at] = (all_rows[i, c, :, at].astype(F32) + other[i, :, at].astype(F32)).astype(BF16)
             if s == 3:
                 for u in range(2):
-                    push(both.at[i, :, half_cols(peers[3], u)], passing.at[u, i], pass_send, pass_recv.at[u, i], here, peers[u + 1])
+                    push(both.at[i, :, half_cols(peers[3], u)], passing.at[u, i], ring_send, pass_recv.at[i], here, peers[u + 1])
             elif s:
                 u = s - 1
-                push(both.at[i, :, half_cols(peers[s], u)], piece_half(s, i, u), half_send, half_recv.at[u, i], here, peers[s])
+                push(both.at[i, :, half_cols(peers[s], u)], piece_half(s, i, u), ring_send, sum_recv.at[i], here, peers[s])
 
     def pass_on(i):
+        arrived(passing.at[:, i], pass_recv.at[i])
         for u in range(2):
             turn = 2 - u
-            arrived(passing.at[u, i], pass_recv.at[u, i])
             passed[u, i] = (passing[u, i].astype(F32) + both[i, :, half_cols(peers[turn], u)].astype(F32)).astype(BF16)
-            push(passed.at[u, i], piece_half(turn, i, u), sum_send, sum_recv.at[turn - 1, i], here, peers[turn])
+            push(passed.at[u, i], piece_half(turn, i, u), ring_send, sum_recv.at[i], here, peers[turn])
 
     def reduce_tp(i):
-        for s in (1, 2):
-            arrived(piece_half(s, i, s - 1), half_recv.at[s - 1, i])
-            arrived(piece_half(s, i, 2 - s), sum_recv.at[s - 1, i])
+        arrived(pieces.at[:, i], sum_recv.at[i])
         acc = both[i, :, cols(t)].astype(F32) + pieces[0, i].astype(F32) + pieces[1, i].astype(F32)
         if i == 0:
             back_rows[z] = acc.astype(BF16)
@@ -688,7 +706,7 @@
     g_tile = min(512, width)
 
     def input_tiles(begin, end):
-        @pl.loop(begin, end)
+        @pl.loop(begin, end, unroll=min(2, end - begin))
         def _(j):
             at = pl.ds(pl.multiple_of(j * g_tile, g_tile), g_tile)
             columns = x_all[:, :, :, at].reshape(zs * rows, g_tile).T
@@ -697,18 +715,17 @@
                 full[at, :] = term.astype(BF16)
                 norms[pl.ds(i, 1), at] = lane_sums(term * term)
 
-        if end == n_in:
-            store(4, gate_full, gate_out)
-            store(5, up_full, up_out)
-
-    def down_tiles():
-        turned = hidden[...].reshape(zs * rows, hid).T
-        folded[...] = jnp.zeros_like(folded)
-
-        @pl.loop(0, width // g_tile)
+    def turn_hidden():
+        hidden_turned[...] = hidden[...].reshape(zs * rows, hid).T
+
+    def down_tiles(begin, end):
+        if begin == 0:
+            folded[...] = jnp.zeros_like(folded)
+
+        @pl.loop(begin, end, unroll=min(2, end - begin))
         def _(j):
             at = pl.ds(pl.multiple_of(j * g_tile, g_tile), g_tile)
-            term = jnp.dot(turned, y_all[:, :, :, at].reshape(zs * rows, g_tile), preferred_element_type=F32)
+            term = jnp.dot(hidden_turned[...], y_all[:, :, :, at].reshape(zs * rows, g_tile), preferred_element_type=F32)
             down_full[:, at] = term.astype(BF16)
             term = term * term
             acc = term[:, :128]
@@ -716,13 +733,12 @@
                 acc = acc + term[:, k * 128:(k + 1) * 128]
             folded[...] += acc
 
-        store(6, down_full, down_out)
-        out_down_norms[...] = jnp.sum(folded[...].T, axis=0, keepdims=True)
-        store(3, out_down_norms, down_norms_out)
+        if end == n_in:
+            out_down_norms[...] = jnp.sum(folded[...].T, axis=0, keepdims=True)
 
     def send_norms():
         for s in range(1, n_tp):
-            push(norms, norm_pieces.at[s], tn_send, tn_recv.at[s], here, peers[s])
+            push(norms, norm_pieces.at[s], tn_send, tn_recv, here, peers[s])
 
     def swap_scores():
         push(scores.at[1 - c], other_scores, cs_send, cs_recv, mate, t)
@@ -731,53 +747,54 @@
         arrived(other_scores, cs_recv)
         both_scores[...] = scores[c] + other_scores[...]
         for s in range(1, n_tp):
-            push(both_scores, score_pieces.at[s], ts_send, ts_recv.at[s], here, peers[s])
+            push(both_scores, score_pieces.at[s], ts_send, ts_recv, here, peers[s])
 
     def home_scores():
         acc = both_scores[...]
+        arrived(score_pieces.at[pl.ds(1, n_tp - 1)], ts_recv)
         for s in range(1, n_tp):
-            arrived(score_pieces.at[s], ts_recv.at[s])
             acc = acc + score_pieces[s]
         total_scores[...] = acc
         for i in range(1, zs):
-            push(total_scores.at[i], back_scores.at[z], es_send, es_recv.at[z], order[i] * 2 + c, t)
+            push(total_scores.at[i], back_scores.at[z], es_send, es_recv, order[i] * 2 + c, t)
         back_scores[z] = total_scores[0]
 
     def close_norms():
         acc = norms[...]
+        arrived(norm_pieces.at[pl.ds(1, n_tp - 1)], tn_recv)
         for s in range(1, n_tp):
-            arrived(norm_pieces.at[s], tn_recv.at[s])
             acc = acc + norm_pieces[s]
         out_norms[...] = acc
-        store(2, out_norms, norms_out)
 
     def close_scores():
-        for q in order[1:]:
-            arrived(back_scores.at[q], es_recv.at[q])
+        arrived(back_scores.at[pl.ds(0, zs - 1)], es_recv)
         for k in range(len(picks)):
             found = jnp.zeros((1, tok), F32)
             for e in range(zs):
                 column = jnp.broadcast_to(back_scores[e], (8, back_scores.shape[2])).T[:cap, :1]
                 found = found + jnp.sum(jnp.where(matches(e)[k], column, 0.0), axis=0, keepdims=True)
             out_mixing[k:k + 1, :] = found / mixing[k:k + 1, :]
-        store(1, out_mixing, mixing_out)
 
     def close_tokens():
-        for q in order[1:]:
-            arrived(back_rows.at[q], home_recv.at[q])
+        last = (2 * z + 1) % 5
         acc = jnp.zeros((tok, part), F32)
-        for e in range(zs):
+        for k in range(1, zs + 1):
+            e = (last + k) % zs
+
+            @pl.when(e != z)
+            def _():
+                arrived(back_rows.at[e], home_recv.at[e])
+
             pick = sum(hit.astype(F32) for hit in matches(e)).astype(BF16)
             acc = acc + lax.dot_general(pick, back_rows[e], first, preferred_element_type=F32)
         out_tokens[...] = acc.astype(BF16)
-        store(0, out_tokens, tokens_out)
 
     n_in = width // g_tile
     cross(1)
-
-    @pl.when(outer == 0)
+    cross(3)
+
+    @pl.when(outer == 1)
     def _():
-        cross(3)
         cross(2)
 
     spread(0)
@@ -788,14 +805,13 @@
     turn_in(1)
     finish(0)
 
-    @pl.when(outer == 1)
+    @pl.when(outer == 0)
     def _():
         cross(2)
-        cross(3)
 
     relay(1)
     forward(0)
-    spread(2)
+    spread(2, True)
     row_terms(0)
     finish(1)
     forward(1)
@@ -804,43 +820,42 @@
     row_terms(1)
     finish(2)
     relay(3)
-    reduce_core(0)
     reduce_core(1)
     forward(2)
     row_terms(2)
     finish(3)
-    pass_on(0)
+    reduce_core(2)
+    pass_on(1)
     forward(3)
     swap_scores()
-    pass_on(1)
-    reduce_core(2)
-    row_terms(3)
+    row_terms(3, (3, 1))
+    pass_on(2)
+    row_terms(3, (2, 0))
     spread_scores()
-    pass_on(2)
+    turn_hidden()
     reduce_core(3)
-    reduce_tp(0)
     reduce_tp(1)
+    reduce_core(0)
     input_tiles(0, n_in // 2)
+    reduce_tp(2)
+    home_scores()
     pass_on(3)
-    home_scores()
-    reduce_tp(2)
     input_tiles(n_in // 2, n_in)
     send_norms()
+    pass_on(0)
+    down_tiles(0, n_in // 2)
     reduce_tp(3)
-    down_tiles()
+    down_tiles(n_in // 2, n_in)
+    reduce_tp(0)
+    close_scores()
     close_norms()
-    close_scores()
     close_tokens()
-    for copy in stores:
-        copy.wait()
-    for a in range(2):
-        arrived(puts[a].at[pl.ds(0, zs - 1)], ep_send.at[a])
-        arrived(alls[a].at[:, 0], core_send.at[a])
-        arrived(alls[a].at[:, 0, :, pl.ds(0, 2 * part)], tp_send.at[a])
-        arrived(alls[a].at[:, 0, :, pl.ds(0, part)], fwd_send.at[a])
+    arrived(x_all.at[pl.ds(0, zs - 1), :, :, pl.ds(0, part)], ep_send)
+    arrived(x_all, core_send)
+    arrived(x_all.at[:, :, :, pl.ds(0, 2 * part)], tp_send)
+    arrived(x_all.at[:, :, :, pl.ds(0, part)], fwd_send)
     arrived(other, swap_send)
-    for sem in (pass_send, half_send, sum_send):
-        arrived(passing, sem)
+    arrived(x_all.at[pl.ds(0, 3), :, :, pl.ds(0, zs * part // 2)], ring_send)
     arrived(total.at[pl.ds(0, zs - 1)], home_send)
     arrived(other_scores, cs_send)
     arrived(score_pieces.at[pl.ds(0, n_tp - 1)], ts_send)
@@ -848,25 +863,31 @@
     arrived(total_scores.at[pl.ds(0, zs - 1)], es_send)
 
 
-def settle_kernel(*refs):
+def settle_kernel(slices, *refs):
     count = len(refs) // 2
     sem = refs[-1]
-    copies = [pltpu.make_async_copy(refs[i], refs[count + i], sem.at[i]) for i in range(count)]
+    copies = []
+    for i in range(count):
+        lines = refs[i].shape[0]
+        parts = slices if lines % (16 * slices) == 0 else 1
+        for k in range(parts):
+            at = pl.ds(k * (lines // parts), lines // parts)
+            copies.append(pltpu.make_async_copy(refs[i].at[at], refs[count + i].at[at], sem.at[i, k]))
     for copy in copies:
         copy.start()
     for copy in copies:
         copy.wait()
 
 
-def settle(arrays):
+def settle(arrays, slices=1):
     far = pl.BlockSpec(memory_space=pltpu.HBM)
     vm = pl.BlockSpec(memory_space=pltpu.VMEM)
     return pl.pallas_call(
-        settle_kernel,
+        functools.partial(settle_kernel, slices),
         out_shape=tuple(jax.ShapeDtypeStruct(a.shape, a.dtype) for a in arrays),
         in_specs=[vm] * len(arrays),
         out_specs=(far,) * len(arrays),
-        scratch_shapes=[pltpu.SemaphoreType.DMA((len(arrays),))],
+        scratch_shapes=[pltpu.SemaphoreType.DMA((len(arrays), slices))],
         compiler_params=pltpu.CompilerParams(vmem_limit_bytes=2 << 20),
         name="settle",
     )(*[pltpu.with_memory_space_constraint(a, pltpu.VMEM) for a in arrays])
@@ -876,7 +897,7 @@
     top, tok = routing.shape
     part = tokens.shape[1]
     width, hid = w_gate.shape
-    anywhere = pl.BlockSpec(memory_space=pl.ANY)
+    vm = pl.BlockSpec(memory_space=pltpu.VMEM)
     far = pl.BlockSpec(memory_space=pltpu.HBM)
     dma = pltpu.SemaphoreType.DMA
     line = -(-cap // 128) * 128
@@ -891,10 +912,8 @@
             room(width, hid), room(width, hid), room(hid, width),
         ),
         in_specs=[far] * 7,
-        out_specs=(anywhere,) * 7,
+        out_specs=(vm,) * 7,
         scratch_shapes=[
-            room(tok, part), room(top, tok, kind=F32), room(2, width, kind=F32), room(1, hid, kind=F32),
-            room(width, hid), room(width, hid), room(hid, width),
             room(top, tok, kind=jnp.int32), room(top, tok, kind=F32), room(tok, part), room(tok, part),
             room(width, hid), room(width, hid), room(hid, width), room(hid, width), room(hid, width), room(width, hid),
             room(zs, cap, part), room(zs, cap, part), room(zs, 2, cap, width), room(zs, 2, cap, width),
@@ -904,11 +923,10 @@
             room(zs, cap, part), room(zs, cap, part),
             room(2, zs, 1, line, kind=F32), room(zs, 1, line, kind=F32), room(zs, 1, line, kind=F32),
             room(n_tp, zs, 1, line, kind=F32), room(zs, 1, line, kind=F32), room(zs, 1, line, kind=F32),
-            room(2, width, kind=F32), room(n_tp, 2, width, kind=F32), room(hid, 128, kind=F32),
-            dma((7,)), dma((7,)), dma((2,)), dma((2,)), dma((2, zs)), dma((2,)), dma((2, zs, n_tp)),
-            dma((2,)), dma((2,)), dma((2, zs, n_tp)),
-            dma, dma((zs, n_tp)), dma, dma((2, zs)), dma, dma((2, zs)), dma, dma((2, zs)),
-            dma, dma, dma, dma((n_tp,)), dma, dma((n_tp,)), dma, dma((zs,)), dma, dma((zs,)),
+            room(2, width, kind=F32), room(n_tp, 2, width, kind=F32), room(hid, 128, kind=F32), room(hid, 2 * zs * cap),
+            dma((7,)), dma, dma, dma((2, zs)), dma, dma((zs, 6)), dma, dma, dma((zs,)),
+            dma, dma((zs, 2)), dma, dma((zs,)), dma((zs,)),
+            dma, dma, dma, dma, dma, dma, dma, dma((zs,)), dma, dma,
         ],
         compiler_params=pltpu.CompilerParams(collective_id=2, has_side_effects=True, vmem_limit_bytes=50 << 20),
         name="fused",

time: 56.9 us -> 50.5 us (0.89)
  Pallas kernels: 56.1 us -> 49.7 us
    pallas_call x1, Pallas kernels: 53.3 us -> 46.9 us  [fused(): pl.pallas_call(functools.partial(fused_kernel, zs, n_tp, part, cap, tok),...]
where the time goes in v2:
time: 50.5 us; the launch traced here: 50.3 us
  Pallas kernels  49.7 us (98%)
  between operations  0.64 us (1%)
    pallas_call x1, Pallas kernels, fused(): pl.pallas_call(functools.partial(fused_kernel, zs, n_tp, part, cap, tok),...  46.9 us
    pallas_call x1, Pallas kernels, settle(): pl.pallas_call(functools.partial(settle_kernel, slices), out_shape=tuple(...  2.82 us

profile of v2, /device:TPU:0, one launch (start us, length us, event | category | flops | bytes accessed | tf_op | source)
XLA Modules:
  0.0 50.3 jit_solution(7035976446223595354)
XLA Ops:
  0.6 46.9 %fused.1 = (bf16[128,512]{1,0:T(8,128)(2,1)S(1)}, f32[2,128]{1,0:T(2,128)S(1)}, f32[2,2048]{1,0:T(2,128)S(1)}, f32[1,512]{1,0:T(1,128)S(1)}, bf16[2048,512]{1,0:...) custom-call(s32[2,128]{1,0:T(2,128)} %bitcast.13, f32[2,128]{1,0:T(2,128)} %bitcast.14, ...), custom_call_target="tpu_custom_call" | custom-call | tf_op jit(solution)/shard_map/fused/pallas_call | solution.py:908
  47.5 2.8 %settle.1 = (bf16[128,512]{1,0:T(8,128)(2,1)}, f32[2,128]{1,0:T(2,128)}, f32[2,2048]{1,0:T(2,128)}, f32[1,512]{1,0:T(1,128)}, bf16[2048,512]{1,0:T(8,128)(2,1)},...) custom-call(bf16[128,512]{1,0:T(8,128)(2,1)S(1)} %get-tuple-element.21.refs_0_, ...), custom_call_target="tpu_custom_call" | custom-call | tf_op jit(solution)/shard_map/settle/pallas_call | solution.py:885

commit v3 on v2

--- a/solution.py
+++ b/solution.py
@@ -533,8 +533,8 @@
     everyone_in()
 
     outer = (z - 1) * (z - 2) // 2
-    order = [z, 1 + z % 2, 3 - 3 * (z // 2), (2 + 3 * z) % 5]
-    lands = [0, 1 + 2 * outer, 3 - outer, 1 + outer]
+    order = [z, 1 + z % 2, 3 - 3 * (z % 2), (z + 2) % zs]
+    lands = [0, 1 + outer, 1 + outer, 3]
     puts, alls = (x_put, y_put), (x_all, y_all)
 
     def block(a, i, core, feat):
@@ -672,8 +672,8 @@
     def piece_half(s, i, u):
         return pieces.at[s - 1, i, :, pl.ds(u * (part // 2), part // 2)]
 
-    def reduce_core(i):
-        for s in (3, 1, 2, 0):
+    def reduce_core(i, steps=(3, 1, 2, 0)):
+        for s in steps:
             at = cols(peers[s])
             if s == 3:
                 arrived(other.at[i, :, at], swap_recv.at[i, 0])
@@ -776,7 +776,7 @@
             out_mixing[k:k + 1, :] = found / mixing[k:k + 1, :]
 
     def close_tokens():
-        last = (2 * z + 1) % 5
+        last = (z + 2) % zs
         acc = jnp.zeros((tok, part), F32)
         for k in range(1, zs + 1):
             e = (last + k) % zs
@@ -791,11 +791,11 @@
 
     n_in = width // g_tile
     cross(1)
-    cross(3)
+    cross(2)
 
     @pl.when(outer == 1)
     def _():
-        cross(2)
+        cross(3)
 
     spread(0)
     turn_down()
@@ -807,11 +807,11 @@
 
     @pl.when(outer == 0)
     def _():
-        cross(2)
+        cross(3)
 
     relay(1)
     forward(0)
-    spread(2, True)
+    spread(2)
     row_terms(0)
     finish(1)
     forward(1)
@@ -830,21 +830,24 @@
     swap_scores()
     row_terms(3, (3, 1))
     pass_on(2)
-    row_terms(3, (2, 0))
+    row_terms(3, (2,))
+    reduce_core(3, (3,))
+    row_terms(3, (0,))
     spread_scores()
     turn_hidden()
-    reduce_core(3)
+    reduce_core(3, (1, 2, 0))
     reduce_tp(1)
+    input_tiles(0, 1)
+    pass_on(3)
+    reduce_tp(2)
     reduce_core(0)
-    input_tiles(0, n_in // 2)
-    reduce_tp(2)
+    input_tiles(1, n_in - 1)
     home_scores()
-    pass_on(3)
-    input_tiles(n_in // 2, n_in)
+    reduce_tp(3)
+    input_tiles(n_in - 1, n_in)
     send_norms()
     pass_on(0)
     down_tiles(0, n_in // 2)
-    reduce_tp(3)
     down_tiles(n_in // 2, n_in)
     reduce_tp(0)
     close_scores()

time: 50.5 us -> 50.5 us (level)
  no operation moved by 1% of the time
where the time goes in v3:
time: 50.5 us; the launch traced here: 50.3 us
  Pallas kernels  49.7 us (98%)
  between operations  0.64 us (1%)
    pallas_call x1, Pallas kernels, fused(): pl.pallas_call(functools.partial(fused_kernel, zs, n_tp, part, cap, tok),...  46.9 us
    pallas_call x1, Pallas kernels, settle(): pl.pallas_call(functools.partial(settle_kernel, slices), out_shape=tuple(...  2.82 us

profile of v3, /device:TPU:0, one launch (start us, length us, event | category | flops | bytes accessed | tf_op | source)
XLA Modules:
  0.0 50.3 jit_solution(12582787841402605753)
XLA Ops:
  0.6 46.9 %fused.1 = (bf16[128,512]{1,0:T(8,128)(2,1)S(1)}, f32[2,128]{1,0:T(2,128)S(1)}, f32[2,2048]{1,0:T(2,128)S(1)}, f32[1,512]{1,0:T(1,128)S(1)}, bf16[2048,512]{1,0:...) custom-call(s32[2,128]{1,0:T(2,128)} %bitcast.13, f32[2,128]{1,0:T(2,128)} %bitcast.14, ...), custom_call_target="tpu_custom_call" | custom-call | tf_op jit(solution)/shard_map/fused/pallas_call | solution.py:911
  47.5 2.8 %settle.1 = (bf16[128,512]{1,0:T(8,128)(2,1)}, f32[2,128]{1,0:T(2,128)}, f32[2,2048]{1,0:T(2,128)}, f32[1,512]{1,0:T(1,128)}, bf16[2048,512]{1,0:T(8,128)(2,1)},...) custom-call(bf16[128,512]{1,0:T(8,128)(2,1)S(1)} %get-tuple-element.21.refs_0_, ...), custom_call_target="tpu_custom_call" | custom-call | tf_op jit(solution)/shard_map/settle/pallas_call | solution.py:888
